TPU v7x, 32 devices: a whole 2x2x4 slice. The times are simulated.
32 devices in a mesh: sp: 8 (over z, y), tp: 4 (over x, core).
Axes of the slice: x: 2, y: 2, z: 4, core: 2. Of those that a mesh axis runs over, the one named last changes fastest.
Arguments:
- inputs: bfloat16 [4096, 2048], P('sp', 'tp'), may hold values from -6 to 6
- norm_gain: float32 [2048], replicated, may hold values from 0.1 to 1.9
- latent_query: bfloat16 [2048, 1536], P(None, 'tp'), may hold values from -2 to 2
- latent_down: bfloat16 [2048, 512], replicated, may hold values from -2 to 2
- rope_down: bfloat16 [2048, 32], replicated, may hold values from -2 to 2
- latent_gain: float32 [512], replicated, may hold values from 0.1 to 1.9
- latent_up: bfloat16 [512, 2048], P(None, 'tp'), may hold values from -2 to 2
- window_query: bfloat16 [2048, 1024], P(None, 'tp'), may hold values from -2 to 2
- window_key: bfloat16 [2048, 512], P(None, 'tp'), may hold values from -2 to 2
- window_value: bfloat16 [2048, 512], P(None, 'tp'), may hold values from -0.125 to 0.125
- sink_logit: float32 [16], P('tp'), may hold values from 3 to 8
- out_latent: bfloat16 [1024, 2048], P('tp'), may hold values from -0.1875 to 0.1875
- out_window: bfloat16 [1024, 2048], P('tp'), may hold values from -0.1875 to 0.1875
Outputs:
- attended: bfloat16 [4096, 2048], P('sp', 'tp')
All inputs are finite; a program needn't handle non-finite values.
Results may differ from a plain program's by a relative error of at most 0.017.
Values may be sent and summed in bfloat16 or wider, within the bound.
A program may use at most 128 MiB of HBM per device.

v0:
```python
import jax
import jax.numpy as jnp
from jax import lax
from jax.sharding import PartitionSpec as P

NOPE = 64
ROPE = 32
HEAD = 64
WINDOW = 128


epsilon = 1e-06
key_block = 512


def with_halo(cells, sides, width):
    for axis, dim in sides:
        count = lax.axis_size(axis)
        ends = count - 1
        head = lax.slice_in_dim(cells, 0, width, axis=dim)
        tail = lax.slice_in_dim(cells, cells.shape[dim] - width, cells.shape[dim], axis=dim)
        cells = jnp.concatenate(
            [
                lax.ppermute(tail, axis, [(i, (i + 1) % count) for i in range(ends)]),
                cells,
                lax.ppermute(head, axis, [((i + 1) % count, i) for i in range(ends)]),
            ],
            axis=dim,
        )
    return cells


def rms_scale(values, gains):
    return values * lax.rsqrt(jnp.mean(values * values, axis=-1, keepdims=True) + epsilon) * gains


def rotary(values, positions):
    half_width = values.shape[-1] // 2
    inverse = 1.0 / 10000.0 ** (
        jnp.arange(0, 2 * half_width, 2).astype(jnp.float32) / (2 * half_width)
    )
    angles = positions[:, None] * inverse[None, :]
    cosine_table = jnp.cos(angles)[:, None, :]
    sine_table = jnp.sin(angles)[:, None, :]
    first_half = values[..., :half_width]
    second_half = values[..., half_width:]
    return jnp.concatenate(
        [
            first_half * cosine_table - second_half * sine_table,
            second_half * cosine_table + first_half * sine_table,
        ],
        axis=-1,
    )


def attend(running, queries, key_data, rope_keys):
    maxima, denoms, totals = running
    head_count = queries.shape[1]
    stacked = key_data.reshape(key_data.shape[0], head_count, NOPE + HEAD)
    scores = jnp.einsum(
        "qhn,khn->hqk", queries[..., :NOPE], stacked[..., :NOPE], preferred_element_type=jnp.float32
    )
    scores = scores + jnp.einsum(
        "qhr,kr->hqk", queries[..., NOPE:], rope_keys, preferred_element_type=jnp.float32
    )
    scores = scores * (NOPE + ROPE) ** (-0.5)
    highest = jnp.maximum(maxima, jnp.max(scores, axis=-1))
    weights = jnp.exp(scores - highest[..., None])
    shrink = jnp.exp(maxima - highest)
    denoms = denoms * shrink + jnp.sum(weights, axis=-1)
    totals = totals * jnp.transpose(shrink)[:, :, None] + jnp.einsum(
        "hqk,khd->qhd",
        weights.astype(jnp.bfloat16),
        stacked[..., NOPE:],
        preferred_element_type=jnp.float32,
    )
    return (highest, denoms, totals)


def attend_rows(running, queries, key_data, rope_keys):
    row_total = key_data.shape[0]

    def advance(state_now, pieces):
        return (attend(state_now, queries, pieces[0], pieces[1]), None)

    sliced = (
        key_data.reshape(row_total // key_block, key_block, key_data.shape[1]),
        rope_keys.reshape(row_total // key_block, key_block, rope_keys.shape[1]),
    )
    running, unused = lax.scan(advance, running, sliced)
    return running


def shards(
    inputs,
    norm_gain,
    latent_query,
    latent_down,
    rope_down,
    latent_gain,
    latent_up,
    window_query,
    window_key,
    window_value,
    sink_logit,
    out_latent,
    out_window,
):
    row_count = inputs.shape[0]
    gathered = lax.all_gather(inputs, "tp", axis=1, tiled=True)
    hidden = rms_scale(gathered.astype(jnp.float32), norm_gain).astype(jnp.bfloat16)
    offset = lax.axis_index("sp") * row_count
    length_all = row_count * lax.axis_size("sp")
    positions = (offset + jnp.arange(row_count)).astype(jnp.float32)
    latent = rms_scale(
        jnp.dot(hidden, latent_down, preferred_element_type=jnp.float32), latent_gain
    ).astype(jnp.bfloat16)
    shared = rotary(
        jnp.dot(hidden, rope_down, preferred_element_type=jnp.float32)[:, None, :], positions
    )[:, 0, :].astype(jnp.bfloat16)
    head_count = latent_up.shape[1] // (NOPE + HEAD)
    queries = jnp.dot(hidden, latent_query, preferred_element_type=jnp.float32).reshape(
        row_count, head_count, NOPE + ROPE
    )
    queries = jnp.concatenate(
        [queries[..., :NOPE], rotary(queries[..., NOPE:], positions)], axis=-1
    ).astype(jnp.bfloat16)
    start_state = (
        jnp.full((head_count, row_count), -jnp.inf, jnp.float32),
        jnp.zeros((head_count, row_count), jnp.float32),
        jnp.zeros((row_count, head_count, HEAD), jnp.float32),
    )
    expanded = jnp.dot(latent, latent_up, preferred_element_type=jnp.float32).astype(jnp.bfloat16)
    maxima, denoms, totals = attend_rows(
        start_state,
        queries,
        lax.all_gather(expanded, "sp", axis=0, tiled=True),
        lax.all_gather(shared, "sp", axis=0, tiled=True),
    )
    latent_out = (
        (totals / jnp.transpose(denoms)[:, :, None])
        .reshape(row_count, head_count * HEAD)
        .astype(jnp.bfloat16)
    )
    window_heads = window_query.shape[1] // HEAD
    key_heads = window_key.shape[1] // HEAD
    group_size = window_heads // key_heads
    window_queries = rotary(
        jnp.dot(hidden, window_query, preferred_element_type=jnp.float32).reshape(
            row_count, window_heads, HEAD
        ),
        positions,
    ).astype(jnp.bfloat16)
    window_keys = rotary(
        jnp.dot(hidden, window_key, preferred_element_type=jnp.float32).reshape(
            row_count, key_heads, HEAD
        ),
        positions,
    ).astype(jnp.bfloat16)
    window_values = jnp.dot(hidden, window_value, preferred_element_type=jnp.float32).astype(
        jnp.bfloat16
    )
    packed = jnp.concatenate(
        [window_keys.reshape(row_count, key_heads * HEAD), window_values], axis=1
    )
    padded = with_halo(packed, (("sp", 0),), WINDOW)
    block_count = row_count // WINDOW
    grid_rows = padded.reshape(block_count + 2, WINDOW, packed.shape[1])
    banded = jnp.concatenate([grid_rows[:-2], grid_rows[1:-1], grid_rows[2:]], axis=1)
    band_keys = banded[..., : key_heads * HEAD].reshape(block_count, 3 * WINDOW, key_heads, HEAD)
    band_values = banded[..., key_heads * HEAD :].reshape(block_count, 3 * WINDOW, key_heads, HEAD)
    query_band = window_queries.reshape(block_count, WINDOW, key_heads, group_size, HEAD)
    scores = jnp.einsum(
        "nqhgd,nkhd->nhgqk", query_band, band_keys, preferred_element_type=jnp.float32
    ) * HEAD ** (-0.5)
    offsets = jnp.arange(3 * WINDOW)[None, :] - jnp.arange(WINDOW)[:, None]
    key_pos = (
        offset
        - WINDOW
        + jnp.arange(block_count)[:, None] * WINDOW
        + jnp.arange(3 * WINDOW)[None, :]
    )
    allowed = ((offsets >= 0) & (offsets <= 2 * WINDOW))[None] & (
        (key_pos >= 0) & (key_pos < length_all)
    )[:, None, :]
    scores = jnp.where(allowed[:, None, None], scores, -jnp.inf)
    sink_table = sink_logit.reshape(key_heads, group_size)[None, :, :, None]
    highest = jnp.maximum(jnp.max(scores, axis=-1), sink_table)
    weights = jnp.exp(scores - highest[..., None])
    denominators = jnp.sum(weights, axis=-1) + jnp.exp(sink_table - highest)
    window_mix = jnp.einsum(
        "nhgqk,nkhd->nqhgd",
        weights.astype(jnp.bfloat16),
        band_values,
        preferred_element_type=jnp.float32,
    )
    window_out = (
        (window_mix / jnp.transpose(denominators, (0, 3, 1, 2))[..., None])
        .reshape(row_count, window_heads * HEAD)
        .astype(jnp.bfloat16)
    )
    contract_dims = (((0,), (1,)), ((), ()))
    own_rows = lax.psum_scatter(
        (
            lax.dot_general(
                out_latent, latent_out, contract_dims, preferred_element_type=jnp.float32
            )
            + lax.dot_general(
                out_window, window_out, contract_dims, preferred_element_type=jnp.float32
            )
        ).astype(jnp.bfloat16),
        "tp",
        scatter_dimension=0,
        tiled=True,
    ).astype(jnp.float32)
    return jnp.transpose(own_rows).astype(jnp.bfloat16)


def solution(mesh):
    in_specs = (
        P("sp", "tp"),
        P(),
        P(None, "tp"),
        P(),
        P(),
        P(),
        P(None, "tp"),
        P(None, "tp"),
        P(None, "tp"),
        P(None, "tp"),
        P("tp"),
        P("tp", None),
        P("tp", None),
    )
    out_specs = P("sp", "tp")
    return jax.shard_map(shards, mesh=mesh, in_specs=in_specs, out_specs=out_specs, check_vma=False)
```

profile of v0, /device:TPU:0, one launch (start us, length us, event | category | flops | bytes accessed | tf_op | source)
XLA Modules:
  0.0 242.7 jit_solution(7290991688203200437)
XLA Ops:
  6.5 0.7 all-gather.4.cloned.1.call-update
  7.3 26.9 %all-gather.4.cloned.1.call-done = bf16[512,2048]{1,0:T(8,128)(2,1)} async-done(((bf16[512,512]{1,0:T(8,128)(2,1)}), bf16[512,2048]{1,0:T(8,128)(2,1)}) %all-gather.4.cloned.1.call-update) | async-done | bytes 2097168 | tf_op jit(solution)/shard_map/all_gather | solution.py:110
  34.2 2.2 fusion.22
  36.5 1.2 fusion.24
  37.8 1.3 multiply_reduce_fusion
  39.2 1.4 convolution_convert_fusion
  40.7 0.6 max.19
  41.5 0.8 multiply_cosine_fusion.2
  42.6 1.0 broadcast_and_fusion
  43.6 2.5 %fusion.72 = f32[512,128]{0,1:T(8,128)S(1)} fusion(bf16[512,2048]{1,0:T(8,128)(2,1)} %copy-done.2, bf16[2048,128]{1,0:T(8,128)(2,1)S(1)} %copy-done.12), kind=kOutput, calls=%fused_computation.117 | convolution fusion | flops 268435456 | bytes 2883584 | tf_op jit(solution)/shard_map/dot_general | solution.py:155
  46.2 0.8 convolution_convert_fusion.1
  47.0 0.7 fusion.53
  47.7 4.0 %collective-permute-start = (bf16[128,256]{0,1:T(8,128)(2,1)}, bf16[128,256]{0,1:T(8,128)(2,1)}, u32[]{:S(2)}, u32[]{:S(2)}) collective-permute-start(bf16[128,256]{0,1:T(8,128)(2,1)} %get-tuple-element.113), channel_id=1, source_target_pairs={{0,4},{4,8},{8,12},{12,16},{16,20},{20,24},{24,28},{1,5},{5,9},{9,... | collective-permute-start | bytes 196616 | tf_op jit(solution)/shard_map/ppermute | solution.py:24
  51.7 1.3 collective-permute-start.1
  53.0 0.8 fusion.73
  53.9 0.7 copy.25
  54.6 0.7 copy.26
  55.3 3.1 %fusion.70 = f32[512,384]{0,1:T(8,128)S(1)} fusion(bf16[512,2048]{1,0:T(8,128)(2,1)} %copy-done.2, bf16[2048,384]{1,0:T(8,128)(2,1)} %param.17), kind=kOutput, calls=%fused_computation.115 | convolution fusion | flops 805306368 | bytes 4456448 | tf_op jit(solution)/shard_map/dot_general | solution.py:122
  58.5 0.7 convolution_bitcast_fusion
  59.4 33.9 %all-gather = bf16[4096,1,32]{0,2,1:T(8,128)(2,1)S(1)} all-gather(bf16[512,1,32]{0,2,1:T(8,128)(2,1)S(1)} %pad_maximum_fusion.7), channel_id=2, replica_groups=mesh['sp'=8,'tp'=4] {'sp'}, dimensions={0}, use_global_device_ids=true | all-gather | bytes 294912 | tf_op jit(solution)/shard_map/all_gather | solution.py:138
  93.4 0.8 copy.22
  94.3 0.9 pad_maximum_fusion.2
  96.5 0.7 fusion.28
  97.3 0.7 fusion.25
  98.1 0.9 fusion.38
  99.0 0.9 copy.28
  99.9 17.7 %all-gather.6.cloned.1.call-done = bf16[4096,512]{1,0:T(8,128)(2,1)} async-done(((bf16[512,512]{1,0:T(8,128)(2,1)}), bf16[4096,512]{1,0:T(8,128)(2,1)}) %all-gather.6.cloned.1.call-update) | async-done | bytes 4194320 | tf_op jit(solution)/shard_map/all_gather | solution.py:137
  117.6 83.2 %while.15 = (s32[]{:T(128)}, f32[4,512]{1,0:T(4,128)S(1)}, f32[4,512]{1,0:T(4,128)}, f32[512,4,64]{0,2,1:T(8,128)}, bf16[8,512,512]{2,1,0:T(8,128)(2,1)}, /*inde...) while((s32[]{:T(128)}, f32[4,512]{1,0:T(4,128)S(1)}, ...), condition=%wide.region_5.6_spmd.clone, body=%wide.region_2.5_spmd.clone.sunk | while | flops 343289856 | bytes 46236408 | solution.py:90
  117.6 1.1 constant_dynamic-slice_fusion.2
  118.9 0.8 fusion.106
  119.7 3.6 %fusion.107 = (f32[4,512]{1,0:T(4,128)S(1)}, f32[4,512,512]{1,2,0:T(8,128)}) fusion(bf16[512,4,96]{0,2,1:T(8,128)(2,1)S(1)} %get-tuple-element.198, bf16[8,512,32]{1,2,0:T(8,128)(2,1)} %get-tuple-element.199, s32[]{:T(128)} %get-tuple-element.184, f32[4,512,512]{2,1,0:T(8,128)S(1)} %fusion.106), kind=kOutput, calls=%fused_computation.113.clone.1 | convolution fusion | flops 70252544 | bytes 8561152 | tf_op jit(solution)/shard_map/while/body/eval_jaxpr/qhr,kr->hqk/dot_general | solution.py:63
  123.3 3.2 %fusion.111 = f32[512,4,64]{0,2,1:T(8,128)S(1)} fusion(f32[4,512,512]{1,2,0:T(8,128)} %get-tuple-element.173, f32[4,512]{1,0:T(4,128)S(1)} %get-tuple-element.194, f32[512,4,64]{0,2,1:T(8,128)S(1)} %copy-done.5, bf16[512,4,128]{0,2,1:T(8,128)(2,1)S(1)} %bitcast.113, f32[512,4]{0,1:T(4,128)S(1)} %get-tuple-element.174, pred[]{:T(512)S(6)} %compare.3), kind=kOutput, calls=%fused_computation.8.clone.1 | convolution fusion | flops 136708096 | bytes 5521409 | tf_op jit(solution)/shard_map/while/body/eval_jaxpr/hqk,khd->qhd/dot_general | solution.py:71
  128.0 1.1 constant_dynamic-slice_fusion.2
  129.3 0.8 fusion.106
  130.1 3.6 %fusion.107 = (f32[4,512]{1,0:T(4,128)S(1)}, f32[4,512,512]{1,2,0:T(8,128)}) fusion(bf16[512,4,96]{0,2,1:T(8,128)(2,1)S(1)} %get-tuple-element.198, bf16[8,512,32]{1,2,0:T(8,128)(2,1)} %get-tuple-element.199, s32[]{:T(128)} %get-tuple-element.184, f32[4,512,512]{2,1,0:T(8,128)S(1)} %fusion.106), kind=kOutput, calls=%fused_computation.113.clone.1 | convolution fusion | flops 70252544 | bytes 8561152 | tf_op jit(solution)/shard_map/while/body/eval_jaxpr/qhr,kr->hqk/dot_general | solution.py:63
  133.7 3.2 %fusion.111 = f32[512,4,64]{0,2,1:T(8,128)S(1)} fusion(f32[4,512,512]{1,2,0:T(8,128)} %get-tuple-element.173, f32[4,512]{1,0:T(4,128)S(1)} %get-tuple-element.194, f32[512,4,64]{0,2,1:T(8,128)S(1)} %copy-done.5, bf16[512,4,128]{0,2,1:T(8,128)(2,1)S(1)} %bitcast.113, f32[512,4]{0,1:T(4,128)S(1)} %get-tuple-element.174, pred[]{:T(512)S(6)} %compare.3), kind=kOutput, calls=%fused_computation.8.clone.1 | convolution fusion | flops 136708096 | bytes 5521409 | tf_op jit(solution)/shard_map/while/body/eval_jaxpr/hqk,khd->qhd/dot_general | solution.py:71
  138.4 1.1 constant_dynamic-slice_fusion.2
  139.7 0.8 fusion.106
  140.5 3.6 %fusion.107 = (f32[4,512]{1,0:T(4,128)S(1)}, f32[4,512,512]{1,2,0:T(8,128)}) fusion(bf16[512,4,96]{0,2,1:T(8,128)(2,1)S(1)} %get-tuple-element.198, bf16[8,512,32]{1,2,0:T(8,128)(2,1)} %get-tuple-element.199, s32[]{:T(128)} %get-tuple-element.184, f32[4,512,512]{2,1,0:T(8,128)S(1)} %fusion.106), kind=kOutput, calls=%fused_computation.113.clone.1 | convolution fusion | flops 70252544 | bytes 8561152 | tf_op jit(solution)/shard_map/while/body/eval_jaxpr/qhr,kr->hqk/dot_general | solution.py:63
  144.1 3.2 %fusion.111 = f32[512,4,64]{0,2,1:T(8,128)S(1)} fusion(f32[4,512,512]{1,2,0:T(8,128)} %get-tuple-element.173, f32[4,512]{1,0:T(4,128)S(1)} %get-tuple-element.194, f32[512,4,64]{0,2,1:T(8,128)S(1)} %copy-done.5, bf16[512,4,128]{0,2,1:T(8,128)(2,1)S(1)} %bitcast.113, f32[512,4]{0,1:T(4,128)S(1)} %get-tuple-element.174, pred[]{:T(512)S(6)} %compare.3), kind=kOutput, calls=%fused_computation.8.clone.1 | convolution fusion | flops 136708096 | bytes 5521409 | tf_op jit(solution)/shard_map/while/body/eval_jaxpr/hqk,khd->qhd/dot_general | solution.py:71
  148.8 1.1 constant_dynamic-slice_fusion.2
  150.1 0.8 fusion.106
  150.9 3.6 %fusion.107 = (f32[4,512]{1,0:T(4,128)S(1)}, f32[4,512,512]{1,2,0:T(8,128)}) fusion(bf16[512,4,96]{0,2,1:T(8,128)(2,1)S(1)} %get-tuple-element.198, bf16[8,512,32]{1,2,0:T(8,128)(2,1)} %get-tuple-element.199, s32[]{:T(128)} %get-tuple-element.184, f32[4,512,512]{2,1,0:T(8,128)S(1)} %fusion.106), kind=kOutput, calls=%fused_computation.113.clone.1 | convolution fusion | flops 70252544 | bytes 8561152 | tf_op jit(solution)/shard_map/while/body/eval_jaxpr/qhr,kr->hqk/dot_general | solution.py:63
  154.5 3.2 %fusion.111 = f32[512,4,64]{0,2,1:T(8,128)S(1)} fusion(f32[4,512,512]{1,2,0:T(8,128)} %get-tuple-element.173, f32[4,512]{1,0:T(4,128)S(1)} %get-tuple-element.194, f32[512,4,64]{0,2,1:T(8,128)S(1)} %copy-done.5, bf16[512,4,128]{0,2,1:T(8,128)(2,1)S(1)} %bitcast.113, f32[512,4]{0,1:T(4,128)S(1)} %get-tuple-element.174, pred[]{:T(512)S(6)} %compare.3), kind=kOutput, calls=%fused_computation.8.clone.1 | convolution fusion | flops 136708096 | bytes 5521409 | tf_op jit(solution)/shard_map/while/body/eval_jaxpr/hqk,khd->qhd/dot_general | solution.py:71
  159.2 1.1 constant_dynamic-slice_fusion.2
  160.5 0.8 fusion.106
  161.3 3.6 %fusion.107 = (f32[4,512]{1,0:T(4,128)S(1)}, f32[4,512,512]{1,2,0:T(8,128)}) fusion(bf16[512,4,96]{0,2,1:T(8,128)(2,1)S(1)} %get-tuple-element.198, bf16[8,512,32]{1,2,0:T(8,128)(2,1)} %get-tuple-element.199, s32[]{:T(128)} %get-tuple-element.184, f32[4,512,512]{2,1,0:T(8,128)S(1)} %fusion.106), kind=kOutput, calls=%fused_computation.113.clone.1 | convolution fusion | flops 70252544 | bytes 8561152 | tf_op jit(solution)/shard_map/while/body/eval_jaxpr/qhr,kr->hqk/dot_general | solution.py:63
  164.9 3.2 %fusion.111 = f32[512,4,64]{0,2,1:T(8,128)S(1)} fusion(f32[4,512,512]{1,2,0:T(8,128)} %get-tuple-element.173, f32[4,512]{1,0:T(4,128)S(1)} %get-tuple-element.194, f32[512,4,64]{0,2,1:T(8,128)S(1)} %copy-done.5, bf16[512,4,128]{0,2,1:T(8,128)(2,1)S(1)} %bitcast.113, f32[512,4]{0,1:T(4,128)S(1)} %get-tuple-element.174, pred[]{:T(512)S(6)} %compare.3), kind=kOutput, calls=%fused_computation.8.clone.1 | convolution fusion | flops 136708096 | bytes 5521409 | tf_op jit(solution)/shard_map/while/body/eval_jaxpr/hqk,khd->qhd/dot_general | solution.py:71
  169.6 1.1 constant_dynamic-slice_fusion.2
  170.9 0.8 fusion.106
  171.7 3.6 %fusion.107 = (f32[4,512]{1,0:T(4,128)S(1)}, f32[4,512,512]{1,2,0:T(8,128)}) fusion(bf16[512,4,96]{0,2,1:T(8,128)(2,1)S(1)} %get-tuple-element.198, bf16[8,512,32]{1,2,0:T(8,128)(2,1)} %get-tuple-element.199, s32[]{:T(128)} %get-tuple-element.184, f32[4,512,512]{2,1,0:T(8,128)S(1)} %fusion.106), kind=kOutput, calls=%fused_computation.113.clone.1 | convolution fusion | flops 70252544 | bytes 8561152 | tf_op jit(solution)/shard_map/while/body/eval_jaxpr/qhr,kr->hqk/dot_general | solution.py:63
  175.3 3.2 %fusion.111 = f32[512,4,64]{0,2,1:T(8,128)S(1)} fusion(f32[4,512,512]{1,2,0:T(8,128)} %get-tuple-element.173, f32[4,512]{1,0:T(4,128)S(1)} %get-tuple-element.194, f32[512,4,64]{0,2,1:T(8,128)S(1)} %copy-done.5, bf16[512,4,128]{0,2,1:T(8,128)(2,1)S(1)} %bitcast.113, f32[512,4]{0,1:T(4,128)S(1)} %get-tuple-element.174, pred[]{:T(512)S(6)} %compare.3), kind=kOutput, calls=%fused_computation.8.clone.1 | convolution fusion | flops 136708096 | bytes 5521409 | tf_op jit(solution)/shard_map/while/body/eval_jaxpr/hqk,khd->qhd/dot_general | solution.py:71
  180.0 1.1 constant_dynamic-slice_fusion.2
  181.3 0.8 fusion.106
  182.1 3.6 %fusion.107 = (f32[4,512]{1,0:T(4,128)S(1)}, f32[4,512,512]{1,2,0:T(8,128)}) fusion(bf16[512,4,96]{0,2,1:T(8,128)(2,1)S(1)} %get-tuple-element.198, bf16[8,512,32]{1,2,0:T(8,128)(2,1)} %get-tuple-element.199, s32[]{:T(128)} %get-tuple-element.184, f32[4,512,512]{2,1,0:T(8,128)S(1)} %fusion.106), kind=kOutput, calls=%fused_computation.113.clone.1 | convolution fusion | flops 70252544 | bytes 8561152 | tf_op jit(solution)/shard_map/while/body/eval_jaxpr/qhr,kr->hqk/dot_general | solution.py:63
  185.7 3.2 %fusion.111 = f32[512,4,64]{0,2,1:T(8,128)S(1)} fusion(f32[4,512,512]{1,2,0:T(8,128)} %get-tuple-element.173, f32[4,512]{1,0:T(4,128)S(1)} %get-tuple-element.194, f32[512,4,64]{0,2,1:T(8,128)S(1)} %copy-done.5, bf16[512,4,128]{0,2,1:T(8,128)(2,1)S(1)} %bitcast.113, f32[512,4]{0,1:T(4,128)S(1)} %get-tuple-element.174, pred[]{:T(512)S(6)} %compare.3), kind=kOutput, calls=%fused_computation.8.clone.1 | convolution fusion | flops 136708096 | bytes 5521409 | tf_op jit(solution)/shard_map/while/body/eval_jaxpr/hqk,khd->qhd/dot_general | solution.py:71
  190.4 1.1 constant_dynamic-slice_fusion.2
  191.7 0.8 fusion.106
  192.5 3.6 %fusion.107 = (f32[4,512]{1,0:T(4,128)S(1)}, f32[4,512,512]{1,2,0:T(8,128)}) fusion(bf16[512,4,96]{0,2,1:T(8,128)(2,1)S(1)} %get-tuple-element.198, bf16[8,512,32]{1,2,0:T(8,128)(2,1)} %get-tuple-element.199, s32[]{:T(128)} %get-tuple-element.184, f32[4,512,512]{2,1,0:T(8,128)S(1)} %fusion.106), kind=kOutput, calls=%fused_computation.113.clone.1 | convolution fusion | flops 70252544 | bytes 8561152 | tf_op jit(solution)/shard_map/while/body/eval_jaxpr/qhr,kr->hqk/dot_general | solution.py:63
  196.1 3.2 %fusion.111 = f32[512,4,64]{0,2,1:T(8,128)S(1)} fusion(f32[4,512,512]{1,2,0:T(8,128)} %get-tuple-element.173, f32[4,512]{1,0:T(4,128)S(1)} %get-tuple-element.194, f32[512,4,64]{0,2,1:T(8,128)S(1)} %copy-done.5, bf16[512,4,128]{0,2,1:T(8,128)(2,1)S(1)} %bitcast.113, f32[512,4]{0,1:T(4,128)S(1)} %get-tuple-element.174, pred[]{:T(512)S(6)} %compare.3), kind=kOutput, calls=%fused_computation.8.clone.1 | convolution fusion | flops 136708096 | bytes 5521409 | tf_op jit(solution)/shard_map/while/body/eval_jaxpr/hqk,khd->qhd/dot_general | solution.py:71
  200.8 1.1 divide_convert_fusion
  202.0 2.1 fusion.71
  204.0 2.1 fusion.27
  206.2 30.0 %reduce-scatter.2.cloned.1.call-done = bf16[512,512]{0,1:T(8,128)(2,1)} async-done(((bf16[2048,512]{0,1:T(8,128)(2,1)}), bf16[512,512]{0,1:T(8,128)(2,1)}) %reduce-scatter.2.cloned.1.call-update) | async-done | bytes 524304 | tf_op jit(solution)/shard_map/reduce_scatter | solution.py:203
  (205 shorter events, 16.6 us)
Async XLA Ops:
  6.5 31.2 %copy-start = (bf16[2048,512]{1,0:T(8,128)(2,1)S(1)}, bf16[2048,512]{1,0:T(8,128)(2,1)}, u32[]{:S(2)}) copy-start(bf16[2048,512]{1,0:T(8,128)(2,1)} %param.18) | copy-start | bytes 6291460
  6.5 27.7 %all-gather.4.cloned.1.call-start = ((), (), s32[]{:S(2)}) async-start(), calls=%async_computation.1 | async-start | bytes 2621440 | tf_op jit(solution)/shard_map/all_gather | solution.py:110
  7.3 110.4 %all-gather.6.cloned.1.call-start = ((), (), s32[]{:S(2)}) async-start(), calls=%async_computation.2 | async-start | bytes 4718592 | tf_op jit(solution)/shard_map/all_gather | solution.py:137
  34.2 2.2 copy-start.7
  37.7 1.4 copy-start.2
  37.7 1.4 copy-start.11
  37.7 1.4 copy-start.24
  37.8 2.9 %copy-start.26 = (f32[4]{0:T(128)S(1)}, f32[4]{0:T(128)}, u32[]{:S(2)}) copy-start(f32[4]{0:T(128)} %param.25) | copy-start | bytes 52
  39.1 4.5 %copy-start.12 = (bf16[2048,128]{1,0:T(8,128)(2,1)S(1)}, bf16[2048,128]{1,0:T(8,128)(2,1)}, u32[]{:S(2)}) copy-start(bf16[2048,128]{1,0:T(8,128)(2,1)} %param.23) | copy-start | bytes 1572868
  39.2 7.0 %copy-start.13 = (bf16[2048,128]{1,0:T(8,128)(2,1)S(1)}, bf16[2048,128]{1,0:T(8,128)(2,1)}, u32[]{:S(2)}) copy-start(bf16[2048,128]{1,0:T(8,128)(2,1)} %param.24) | copy-start | bytes 1572868
  40.6 195.6 %reduce-scatter.2.cloned.1.call-start = ((), (), s32[]{:S(2)}) async-start(), calls=%async_computation.3 | async-start | bytes 2621440 | tf_op jit(solution)/shard_map/reduce_scatter | solution.py:203
  41.3 4.8 %copy-start.3 = (bf16[512,2048]{1,0:T(8,128)(2,1)S(1)}, bf16[512,2048]{1,0:T(8,128)(2,1)}, u32[]{:S(2)}) copy-start(bf16[512,2048]{1,0:T(8,128)(2,1)} %copy-done.2) | copy-start | bytes 6291460
  41.3 5.7 %copy-start.22 = (f32[16]{0:T(128)}, f32[16]{0:T(128)S(1)}, u32[]{:S(2)}) copy-start(f32[16]{0:T(128)S(1)} %negate_power_fusion.1) | copy-start | bytes 196
  43.6 9.4 %copy-start.25 = (bf16[2048,256]{1,0:T(8,128)(2,1)S(1)}, bf16[2048,256]{1,0:T(8,128)(2,1)}, u32[]{:S(2)}) copy-start(bf16[2048,256]{1,0:T(8,128)(2,1)} %param.22) | copy-start | bytes 3145732
  47.7 46.6 %collective-permute-start = (bf16[128,256]{0,1:T(8,128)(2,1)}, bf16[128,256]{0,1:T(8,128)(2,1)}, u32[]{:S(2)}, u32[]{:S(2)}) collective-permute-start(bf16[128,256]{0,1:T(8,128)(2,1)} %get-tuple-element.113), channel_id=1, source_target_pairs={{0,4},{4,8},{8,12},{12,16},{16,20},{20,24},{24,28},{1,5},{5,9},{9,... | collective-permute-start | bytes 196616 | tf_op jit(solution)/shard_map/ppermute | solution.py:24
  51.7 42.7 %collective-permute-start.1 = (bf16[128,256]{0,1:T(8,128)(2,1)}, bf16[128,256]{0,1:T(8,128)(2,1)}, u32[]{:S(2)}, u32[]{:S(2)}) collective-permute-start(bf16[128,256]{0,1:T(8,128)(2,1)} %get-tuple-element.112), channel_id=1, source_target_pairs={{4,0},{8,4},{12,8},{16,12},{20,16},{24,20},{28,24},{5,1},{9,5},{13... | collective-permute-start | bytes 196616 | tf_op jit(solution)/shard_map/ppermute | solution.py:26
  54.6 3.9 %copy-start.4 = (bf16[512,2048]{1,0:T(8,128)(2,1)S(1)}, bf16[512,2048]{1,0:T(8,128)(2,1)}, u32[]{:S(2)}) copy-start(bf16[512,2048]{1,0:T(8,128)(2,1)} %copy-done.2) | copy-start | bytes 6291460
  54.6 3.9 %copy-start.18 = (bf16[2048,32]{0,1:T(8,128)(2,1)S(1)}, bf16[2048,32]{0,1:T(8,128)(2,1)}, u32[]{:S(2)}) copy-start(bf16[2048,32]{0,1:T(8,128)(2,1)} %param.19) | copy-start | bytes 393220
  55.2 3.9 %copy-start.23 = (f32[16]{0:T(128)S(1)}, f32[16]{0:T(128)}, u32[]{:S(2)}) copy-start(f32[16]{0:T(128)} %copy-done.22) | copy-start | bytes 196
  58.4 35.9 %copy-start.16 = (f32[512,16]{0,1:T(8,128)S(1)}, f32[512,16]{0,1:T(8,128)}, u32[]{:S(2)}) copy-start(f32[512,16]{0,1:T(8,128)} %get-tuple-element.118) | copy-start | bytes 98308
  58.4 35.8 %copy-start.17 = (f32[512,16]{0,1:T(8,128)S(1)}, f32[512,16]{0,1:T(8,128)}, u32[]{:S(2)}) copy-start(f32[512,16]{0,1:T(8,128)} %get-tuple-element.119) | copy-start | bytes 98308
  95.5 0.9 copy-start.10
  95.5 1.0 copy-start.19
  95.5 1.0 copy-start.20
  96.3 1.0 copy-start.21
  119.7 3.6 %copy-start.5 = (f32[512,4,64]{0,2,1:T(8,128)S(1)}, f32[512,4,64]{0,2,1:T(8,128)}, u32[]{:S(2)}) copy-start(f32[512,4,64]{0,2,1:T(8,128)} %get-tuple-element.187) | copy-start | bytes 1572868 | tf_op jit(solution)/shard_map/while
  123.3 3.4 %copy-start.1 = (f32[4,512,512]{1,2,0:T(8,128)S(1)}, f32[4,512,512]{1,2,0:T(8,128)}, u32[]{:S(2)}) copy-start(f32[4,512,512]{1,2,0:T(8,128)} %get-tuple-element.173) | copy-start | bytes 12582916 | tf_op jit(solution)/shard_map/while
  126.7 0.8 copy-start.6
  126.7 0.7 copy-start.14
  127.4 0.6 copy-start.15
  130.1 3.6 %copy-start.5 = (f32[512,4,64]{0,2,1:T(8,128)S(1)}, f32[512,4,64]{0,2,1:T(8,128)}, u32[]{:S(2)}) copy-start(f32[512,4,64]{0,2,1:T(8,128)} %get-tuple-element.187) | copy-start | bytes 1572868 | tf_op jit(solution)/shard_map/while
  133.7 3.4 %copy-start.1 = (f32[4,512,512]{1,2,0:T(8,128)S(1)}, f32[4,512,512]{1,2,0:T(8,128)}, u32[]{:S(2)}) copy-start(f32[4,512,512]{1,2,0:T(8,128)} %get-tuple-element.173) | copy-start | bytes 12582916 | tf_op jit(solution)/shard_map/while
  137.1 0.8 copy-start.6
  137.1 0.7 copy-start.14
  140.5 3.6 %copy-start.5 = (f32[512,4,64]{0,2,1:T(8,128)S(1)}, f32[512,4,64]{0,2,1:T(8,128)}, u32[]{:S(2)}) copy-start(f32[512,4,64]{0,2,1:T(8,128)} %get-tuple-element.187) | copy-start | bytes 1572868 | tf_op jit(solution)/shard_map/while
  144.1 3.4 %copy-start.1 = (f32[4,512,512]{1,2,0:T(8,128)S(1)}, f32[4,512,512]{1,2,0:T(8,128)}, u32[]{:S(2)}) copy-start(f32[4,512,512]{1,2,0:T(8,128)} %get-tuple-element.173) | copy-start | bytes 12582916 | tf_op jit(solution)/shard_map/while
  147.5 0.8 copy-start.6
  147.5 0.7 copy-start.14
  148.2 0.6 copy-start.15
  150.9 3.6 %copy-start.5 = (f32[512,4,64]{0,2,1:T(8,128)S(1)}, f32[512,4,64]{0,2,1:T(8,128)}, u32[]{:S(2)}) copy-start(f32[512,4,64]{0,2,1:T(8,128)} %get-tuple-element.187) | copy-start | bytes 1572868 | tf_op jit(solution)/shard_map/while
  154.5 3.4 %copy-start.1 = (f32[4,512,512]{1,2,0:T(8,128)S(1)}, f32[4,512,512]{1,2,0:T(8,128)}, u32[]{:S(2)}) copy-start(f32[4,512,512]{1,2,0:T(8,128)} %get-tuple-element.173) | copy-start | bytes 12582916 | tf_op jit(solution)/shard_map/while
  157.9 0.8 copy-start.6
  157.9 0.7 copy-start.14
  158.6 0.6 copy-start.15
  161.3 3.6 %copy-start.5 = (f32[512,4,64]{0,2,1:T(8,128)S(1)}, f32[512,4,64]{0,2,1:T(8,128)}, u32[]{:S(2)}) copy-start(f32[512,4,64]{0,2,1:T(8,128)} %get-tuple-element.187) | copy-start | bytes 1572868 | tf_op jit(solution)/shard_map/while
  164.9 3.4 %copy-start.1 = (f32[4,512,512]{1,2,0:T(8,128)S(1)}, f32[4,512,512]{1,2,0:T(8,128)}, u32[]{:S(2)}) copy-start(f32[4,512,512]{1,2,0:T(8,128)} %get-tuple-element.173) | copy-start | bytes 12582916 | tf_op jit(solution)/shard_map/while
  168.3 0.8 copy-start.6
  168.3 0.7 copy-start.14
  171.7 3.6 %copy-start.5 = (f32[512,4,64]{0,2,1:T(8,128)S(1)}, f32[512,4,64]{0,2,1:T(8,128)}, u32[]{:S(2)}) copy-start(f32[512,4,64]{0,2,1:T(8,128)} %get-tuple-element.187) | copy-start | bytes 1572868 | tf_op jit(solution)/shard_map/while
  175.3 3.4 %copy-start.1 = (f32[4,512,512]{1,2,0:T(8,128)S(1)}, f32[4,512,512]{1,2,0:T(8,128)}, u32[]{:S(2)}) copy-start(f32[4,512,512]{1,2,0:T(8,128)} %get-tuple-element.173) | copy-start | bytes 12582916 | tf_op jit(solution)/shard_map/while
  178.7 0.8 copy-start.6
  178.7 0.7 copy-start.14
  179.4 0.6 copy-start.15
  182.1 3.6 %copy-start.5 = (f32[512,4,64]{0,2,1:T(8,128)S(1)}, f32[512,4,64]{0,2,1:T(8,128)}, u32[]{:S(2)}) copy-start(f32[512,4,64]{0,2,1:T(8,128)} %get-tuple-element.187) | copy-start | bytes 1572868 | tf_op jit(solution)/shard_map/while
  185.7 3.4 %copy-start.1 = (f32[4,512,512]{1,2,0:T(8,128)S(1)}, f32[4,512,512]{1,2,0:T(8,128)}, u32[]{:S(2)}) copy-start(f32[4,512,512]{1,2,0:T(8,128)} %get-tuple-element.173) | copy-start | bytes 12582916 | tf_op jit(solution)/shard_map/while
  189.1 0.8 copy-start.6
  189.1 0.7 copy-start.14
  189.8 0.6 copy-start.15
  192.5 3.6 %copy-start.5 = (f32[512,4,64]{0,2,1:T(8,128)S(1)}, f32[512,4,64]{0,2,1:T(8,128)}, u32[]{:S(2)}) copy-start(f32[512,4,64]{0,2,1:T(8,128)} %get-tuple-element.187) | copy-start | bytes 1572868 | tf_op jit(solution)/shard_map/while
  196.1 3.4 %copy-start.1 = (f32[4,512,512]{1,2,0:T(8,128)S(1)}, f32[4,512,512]{1,2,0:T(8,128)}, u32[]{:S(2)}) copy-start(f32[4,512,512]{1,2,0:T(8,128)} %get-tuple-element.173) | copy-start | bytes 12582916 | tf_op jit(solution)/shard_map/while
  199.5 0.8 copy-start.6
  199.5 0.7 copy-start.14
  201.9 2.1 copy-start.8
  201.9 2.1 copy-start.9
  (3 other events, 1.8 us)
Sparse Core Ops, SparseCore 0:
  8.9 25.2 all-gather.3
  40.7 76.8 all-gather.5
  206.3 29.8 reduce-scatter.1
where the time goes:
time: 244 us; the launch traced here: 243 us
  matrix products  76.4 us (31%)
  waiting for transfers between devices  75.4 us (31%)
  blocking collectives  33.9 us (14%)
  local copies, waits for them, and re-layouts  23 us (9%)
  other arithmetic  14.5 us (6%)
  between operations  13.6 us (6%)
  starting transfers between devices  5.35 us (2%)
    all_gather x1, blocking collectives, shards(): lax.all_gather(shared, 'sp', axis=0, tiled=True)  33.9 us
    reduce_scatter x1, waiting for transfers between devices, shards(): lax.psum_scatter((lax.dot_general(out_latent, latent_out, contract_dims,...  30 us
    dot_general x8, matrix products, attend(): jnp.einsum('qhr,kr->hqk', queries[..., NOPE:], rope_keys, preferred_eleme...  28.6 us
    all_gather x1, waiting for transfers between devices, shards(): gathered = lax.all_gather(inputs, 'tp', axis=1, tiled=True)  26.9 us
    dot_general x8, matrix products, attend(): jnp.einsum('hqk,khd->qhd', weights.astype(jnp.bfloat16), stacked[..., NOP...  25.5 us
    all_gather x1, waiting for transfers between devices, shards(): lax.all_gather(expanded, 'sp', axis=0, tiled=True)  17.7 us
    dynamic_slice x16, local copies, waits for them, and re-layouts, attend_rows(): running, unused = lax.scan(advance, running, sliced)  10.3 us
    while x88, local copies, waits for them, and re-layouts  7.46 us
  transfers between devices with their start and end apart: 5, of which 3 were waited for; matrix products, arithmetic and copies ran while one was open for 8% of the time, Pallas kernels for 0%

commit v1 on v0

v1 whole, which is shorter than its diff:
```python
import functools
import math

import jax
import jax.numpy as jnp
import numpy as np
from jax import lax
from jax.experimental import pallas as pl
from jax.experimental.pallas import tpu as pltpu
from jax.sharding import PartitionSpec as P

NOPE = 64
ROPE = 32
HEAD = 64
WINDOW = 128
EPS = 1e-06
LOG2E = math.log2(math.e)
F32 = jnp.float32
BF16 = jnp.bfloat16
CH = 128


def ring_tables(count):
    bits = count.bit_length() - 1
    ny = 2 ** (bits // 2)
    nz = count // ny
    order = [z * ny for z in range(nz)]
    for step, z in enumerate(reversed(range(nz))):
        row = [z * ny + y for y in range(1, ny)]
        order += row if step % 2 == 0 else row[::-1]
    return ny, nz, order


def cycle_position(s, ny, nz):
    z, y = s // ny, s % ny
    step = nz - 1 - z
    even = step % 2 == 0
    inner = jnp.where(even, y - 1, ny - 1 - y)
    return jnp.where(y == 0, z, nz + step * (ny - 1) + inner)


def cycle_member(p, ny, nz):
    q = jnp.maximum(p - nz, 0)
    step = q // (ny - 1)
    inner = q % (ny - 1)
    y = jnp.where(step % 2 == 0, inner + 1, ny - 1 - inner)
    return jnp.where(p < nz, p * ny, (nz - 1 - step) * ny + y)


def rotate(v, cos, sin):
    half = v.shape[-1] // 2
    a, b = v[:, :half], v[:, half:]
    return jnp.concatenate([a * cos - b * sin, b * cos + a * sin], axis=-1)


def body(dims, *refs):
    (n_sp, n_tp, rows, feat, heads, wheads, kheads) = dims
    (x_ref, gain_ref, lq_h, ld_h, rd_h, lgain_ref, lu_h, wq_h, wk_h, wv_h, sink_ref,
     ol_h, ow_h, cp_ref, cq_ref, off_ref, out_ref,
     lq, ld, rd, lu, wq, wk, wv, ol, ow, xg, hid, lat, krt, qs, qw, wkb, wvb,
     kop, vop, acc, mx, oml, omw, part_p, part_m, prec, xs, xr,
     wsem, xsend, xrecv, xfsend, lsend, lrecv, lfsend, ksend, krecv, kfsend,
     hsend, hrecv, psend, precv, ssend, srecv) = refs
    nr = rows // CH
    nx = n_tp // 2
    group = wheads // kheads
    sp = lax.axis_index("sp")
    tp = lax.axis_index("tp")
    xi, core = tp // 2, tp % 2
    mate = xi * 2 + (1 - core)
    ny, nz, _ = ring_tables(n_sp)
    pos = cycle_position(sp, ny, nz)

    def member(delta):
        return cycle_member(lax.rem(pos + delta + n_sp, n_sp), ny, nz)

    right, left = member(1), member(-1)
    above, below = lax.rem(sp + 1, n_sp), lax.rem(sp + n_sp - 1, n_sp)

    def at(s=None, t=None):
        return {"sp": sp if s is None else s, "tp": tp if t is None else t}

    def rcopy(src, dst, ss, rs, dev):
        return pltpu.make_async_remote_copy(
            src_ref=src, dst_ref=dst, send_sem=ss, recv_sem=rs,
            device_id=dev, device_id_type=pl.DeviceIdType.MESH)

    weights = [pltpu.make_async_copy(h, v, wsem.at[i]) for i, (h, v) in enumerate(
        [(ld_h, ld), (rd_h, rd), (lq_h, lq), (wq_h, wq), (wk_h, wk), (wv_h, wv),
         (lu_h, lu), (ol_h, ol), (ow_h, ow)])]
    for w in weights:
        w.start()

    def xpeer(dx):
        return lax.rem(xi + dx, nx)

    barrier = pltpu.get_barrier_semaphore()
    peers = [at(t=xpeer(dx) * 2 + core) for dx in range(1, nx)]
    peers += [at(t=mate), at(s=right), at(s=left), at(s=above), at(s=below)]
    for dev in peers:
        pl.semaphore_signal(barrier, inc=1, device_id=dev, device_id_type=pl.DeviceIdType.MESH)
    pl.semaphore_wait(barrier, len(peers))

    def xsrc(r):
        return x_ref.at[pl.ds(pl.multiple_of(r * CH, CH), CH)]

    def xcopy(r, dx):
        return rcopy(xsrc(r), xg.at[tp, r], xsend.at[dx, r], xrecv.at[tp, r],
                     at(t=xpeer(dx) * 2 + core))

    def xmate(r):
        return rcopy(xsrc(r), xg.at[tp, r], xsend.at[0, r], xrecv.at[tp, r], at(t=mate))

    def xforward(r, dx):
        src = xpeer(dx) * 2 + core
        return rcopy(xg.at[src, r], xg.at[src, r], xfsend.at[dx, r], xrecv.at[src, r], at(t=mate))

    def xwait(src, r):
        rcopy(xg.at[src, r], xg.at[src, r], xsend.at[0, r], xrecv.at[src, r],
              at(t=mate)).wait_recv()

    def start_x(r, _):
        for dx in range(1, nx):
            xcopy(r, dx).start()
        xmate(r).start()
        return 0

    lax.fori_loop(0, nr, start_x, 0)
    for w in weights[:6]:
        w.wait()

    def uslot(b, r):
        return lat.at[b, r], krt.at[b, r]

    def ring_copies(b, r, way, dev):
        j = r // 2
        l, k = uslot(b, r)
        return [rcopy(l, l, lsend.at[way, b, j], lrecv.at[b, r], dev),
                rcopy(k, k, ksend.at[way, b, j], krecv.at[b, r], dev)]

    def mate_copies(b, r):
        j = r // 2
        l, k = uslot(b, r)
        return [rcopy(l, l, lfsend.at[b, j], lrecv.at[b, r], at(t=mate)),
                rcopy(k, k, kfsend.at[b, j], krecv.at[b, r], at(t=mate))]

    def halo(i):
        src = 1 if i == 0 else nr
        dst = nr + 1 if i == 0 else 0
        dev = at(s=below) if i == 0 else at(s=above)
        return [rcopy(wkb.at[src], wkb.at[dst], hsend.at[i, 0], hrecv.at[i, 0], dev),
                rcopy(wvb.at[src], wvb.at[dst], hsend.at[i, 1], hrecv.at[i, 1], dev)]

    def project(r):
        span = pl.ds(pl.multiple_of(r * CH, CH), CH)
        ssq = jnp.zeros((CH, 1), F32)
        for t in range(n_tp):
            xf = xg[t, r].astype(F32)
            ssq = ssq + jnp.sum(xf * xf, axis=-1, keepdims=True)
            hid[:, t * feat:(t + 1) * feat] = (
                xf * gain_ref[:, t * feat:(t + 1) * feat]).astype(BF16)
        scale = lax.rsqrt(ssq / (n_tp * feat) + EPS)
        tab = cp_ref[span, :] * off_ref[sp, 0:1, :] + cq_ref[span, :] * off_ref[sp, 1:2, :]
        cos_w, sin_w = tab[:, 0:32], tab[:, 32:64]
        cos_l, sin_l = tab[:, 64:80], tab[:, 80:96]
        low = jnp.dot(hid[...], ld[...], preferred_element_type=F32) * scale
        low = low * lax.rsqrt(jnp.mean(low * low, axis=-1, keepdims=True) + EPS) * lgain_ref[...]
        lat[sp, r] = low.astype(BF16)
        shared = jnp.dot(hid[...], rd[...], preferred_element_type=F32) * scale
        shared = rotate(shared, cos_l, sin_l)
        wide = jnp.concatenate([shared, jnp.zeros((CH, CH - ROPE), F32)], axis=-1)
        krt[sp, r] = wide.T[:ROPE].astype(BF16)

        @pl.when(r % 2 == core)
        def _():
            for c in ring_copies(sp, r, 0, at(s=right)) + ring_copies(sp, r, 1, at(s=left)):
                c.start()

        keys = jnp.dot(hid[...], wk[...], preferred_element_type=F32) * scale
        keys = jnp.concatenate(
            [rotate(keys[:, g * HEAD:(g + 1) * HEAD], cos_w, sin_w) for g in range(kheads)], axis=-1)
        wkb[r + 1] = keys.astype(BF16)
        wvb[r + 1] = (jnp.dot(hid[...], wv[...], preferred_element_type=F32) * scale).astype(BF16)

        @pl.when(r == 0)
        def _():
            for c in halo(0):
                c.start()

        @pl.when(r == nr - 1)
        def _():
            for c in halo(1):
                c.start()

        q = jnp.dot(hid[...], lq[...], preferred_element_type=F32) * (
            scale * ((NOPE + ROPE) ** -0.5 * LOG2E))
        width = NOPE + ROPE
        for h in range(heads):
            qh = q[:, h * width:(h + 1) * width]
            qs[h, span, :] = jnp.concatenate(
                [qh[:, :NOPE], rotate(qh[:, NOPE:], cos_l, sin_l),
                 jnp.zeros((CH, 128 - width), F32)], axis=-1).astype(BF16)
        q = jnp.dot(hid[...], wq[...], preferred_element_type=F32) * (
            scale * (HEAD ** -0.5 * LOG2E))
        for g in range(wheads):
            qh = rotate(q[:, g * HEAD:(g + 1) * HEAD], cos_w, sin_w)
            kv = g // group
            pieces = [qh if i == kv else jnp.zeros_like(qh) for i in range(kheads)]
            qw[g, span, :] = jnp.concatenate(pieces, axis=-1).astype(BF16)

    def gather_step(e, _):
        @pl.when(e < nr)
        def _():
            r = e
            xg[tp, r] = x_ref[pl.ds(pl.multiple_of(r * CH, CH), CH), :]
            for dx in range(1, nx):
                xwait(xpeer(dx) * 2 + core, r)
                xforward(r, dx).start()

        @pl.when(e >= 1)
        def _():
            r = e - 1
            for dx in range(nx):
                xwait(xpeer(dx) * 2 + 1 - core, r)
            project(r)
        return 0

    lax.fori_loop(0, nr + 1, gather_step, 0)
    weights[6].wait()

    acc[...] = jnp.zeros_like(acc)
    mx[...] = jnp.full_like(mx, -1e30)
    lane = lax.broadcasted_iota(jnp.int32, (CH, CH), 1)

    def block(b):
        def expand(r, _):
            e = jnp.dot(lat[b, r], lu[...], preferred_element_type=F32)
            kt = jnp.concatenate(
                [jnp.zeros((NOPE, CH), F32), krt[b, r].astype(F32),
                 jnp.zeros((128 - NOPE - ROPE, CH), F32)], axis=0).T
            span = pl.ds(pl.multiple_of(r * CH, CH), CH)
            for h in range(heads):
                eh = e[:, h * 128:(h + 1) * 128]
                kop[h, span, :] = jnp.where(lane < NOPE, eh, kt).astype(BF16)
                vop[h, span, :] = jnp.where(lane < NOPE, 1.0, eh).astype(BF16)
            return 0

        lax.fori_loop(0, nr, expand, 0)
        qt = 256
        tiles = rows // qt

        def tile(i, _):
            h, t = i // tiles, i % tiles
            span = pl.ds(pl.multiple_of(t * qt, qt), qt)
            s = lax.dot_general(qs[h, span, :], kop[h], (((1,), (1,)), ((), ())),
                                preferred_element_type=F32)
            old = mx[h, span, :]
            new = jnp.maximum(old, jnp.max(s, axis=-1, keepdims=True))
            p = jnp.exp2(s - new[:, 0:1]).astype(BF16)
            acc[h, span, :] = acc[h, span, :] * jnp.exp2(old - new) + jnp.dot(
                p, vop[h], preferred_element_type=F32)
            mx[h, span, :] = new
            return 0

        lax.fori_loop(0, heads * tiles, tile, 0)

    def window():
        for i in range(2):
            for c in halo(i):
                c.wait_recv()

        def one(n, _):
            kk = wkb[pl.ds(n, 3)].reshape(3 * CH, wkb.shape[-1])
            vv = wvb[pl.ds(n, 3)].reshape(3 * CH, wvb.shape[-1])
            qi = lax.broadcasted_iota(jnp.int32, (CH, 3 * CH), 0)
            ki = lax.broadcasted_iota(jnp.int32, (CH, 3 * CH), 1)
            kp = sp * rows + (n - 1) * CH + ki
            ok = (ki - qi >= 0) & (ki - qi <= 2 * WINDOW) & (kp >= 0) & (kp < n_sp * rows)
            span = pl.ds(pl.multiple_of(n * CH, CH), CH)
            outs = []
            for g in range(wheads):
                kv = g // group
                s = lax.dot_general(qw[g, span, :], kk, (((1,), (1,)), ((), ())),
                                    preferred_element_type=F32)
                s = jnp.where(ok, s, -1e30)
                sink = sink_ref[0:1, g:g + 1] * LOG2E
                m = jnp.maximum(jnp.max(s, axis=-1, keepdims=True), sink)
                p = jnp.exp2(s - m)
                den = jnp.sum(p, axis=-1, keepdims=True) + jnp.exp2(sink - m)
                o = jnp.dot(p.astype(BF16), vv, preferred_element_type=F32) / den
                outs.append(o[:, kv * HEAD:(kv + 1) * HEAD])
            omw[span, :] = jnp.concatenate(outs, axis=-1).astype(BF16)
            return 0

        lax.fori_loop(0, nr, one, 0)

    half = n_sp // 2

    def ring_step(e, _):
        d, j = e // 2 + 1, e % 2
        r = 2 * j + core
        for way in range(2):
            last = half - core if way == 0 else half - 1 + core
            b = member(-d) if way == 0 else member(d)
            dev = at(s=right) if way == 0 else at(s=left)

            @pl.when((e < n_sp) & (d <= last))
            def _():
                for c in ring_copies(b, r, way, dev):
                    c.wait_recv()

                @pl.when(d < last)
                def _():
                    for c in ring_copies(b, r, way, dev):
                        c.start()

                for c in mate_copies(b, r):
                    c.start()

        d1 = e // 2
        b = jnp.where(e == 0, sp, jnp.where(j == 0, member(-d1), member(d1)))

        @pl.when(e >= 2)
        def _():
            for i in range(nr // 2):
                for c in mate_copies(b, 2 * i + 1 - core):
                    c.wait_recv()

        @pl.when(e == 1)
        def _():
            window()

        @pl.when(e != 1)
        def _():
            block(b)
        return 0

    lax.fori_loop(0, n_sp + 1, ring_step, 0)
    weights[7].wait()
    weights[8].wait()

    for i in range(heads // 2):
        def norm(h):
            a = acc[h]
            return a, pltpu.roll(a, NOPE, 1)
        a0, b0 = norm(2 * i)
        a1, b1 = norm(2 * i + 1)
        low = lax.broadcasted_iota(jnp.int32, a0.shape, 1) < NOPE
        oml[:, i * 128:(i + 1) * 128] = (
            jnp.where(low, b0, a1) / jnp.where(low, a0, b1)).astype(BF16)

    def pcopy(r, k):
        return rcopy(part_p.at[k, r], prec.at[k, r], psend.at[k, r], precv.at[k, r], at(t=mate))

    def scopy(r, dx):
        k = xpeer(dx)
        return rcopy(xs.at[dx, r], xr.at[dx, r], ssend.at[dx, r], srecv.at[dx, r],
                     at(t=k * 2 + core))

    def partial(r, t):
        span = pl.ds(pl.multiple_of(r * CH, CH), CH)
        cols = pl.ds(pl.multiple_of(t * feat, 128), feat)
        return jnp.dot(oml[span, :], ol[:, cols], preferred_element_type=F32) + jnp.dot(
            omw[span, :], ow[:, cols], preferred_element_type=F32)

    def scatter_step(e, _):
        @pl.when(e < nr)
        def _():
            for k in range(nx):
                part_p[k, e] = partial(e, 2 * k + 1 - core).astype(BF16)
                pcopy(e, k).start()
            for k in range(nx):
                part_m[k, e] = partial(e, 2 * k + core)

        @pl.when(e >= 1)
        def _():
            r = e - 1
            for k in range(nx):
                pcopy(r, k).wait_recv()
            for dx in range(1, nx):
                k = xpeer(dx)
                xs[dx, r] = (part_m[k, r] + prec[k, r].astype(F32)).astype(BF16)
                scopy(r, dx).start()
        return 0

    lax.fori_loop(0, nr + 1, scatter_step, 0)

    def final_step(r, _):
        total = part_m[xi, r] + prec[xi, r].astype(F32)
        for dx in range(1, nx):
            scopy(r, dx).wait_recv()
            total = total + xr[dx, r].astype(F32)
        out_ref[pl.ds(pl.multiple_of(r * CH, CH), CH), :] = total.astype(BF16)
        return 0

    lax.fori_loop(0, nr, final_step, 0)

    def drain_rows(r, _):
        xmate(r).wait_send()
        for dx in range(1, nx):
            xcopy(r, dx).wait_send()
            xforward(r, dx).wait_send()
            scopy(r, dx).wait_send()
        for k in range(nx):
            pcopy(r, k).wait_send()
        return 0

    lax.fori_loop(0, nr, drain_rows, 0)
    for i in range(2):
        for c in halo(i):
            c.wait_send()

    def drain_ring(e, _):
        d, j = e // 2, e % 2
        r = 2 * j + core
        for way in range(2):
            last = half - core if way == 0 else half - 1 + core
            b = member(-d) if way == 0 else member(d)
            dev = at(s=right) if way == 0 else at(s=left)

            @pl.when(d < last)
            def _():
                for c in ring_copies(b, r, way, dev):
                    c.wait_send()

            @pl.when((d >= 1) & (d <= last))
            def _():
                for c in mate_copies(b, r):
                    c.wait_send()
        return 0

    lax.fori_loop(0, n_sp + 2, drain_ring, 0)


def tables(rows, n_sp):
    freq_w = 10000.0 ** (-np.arange(32) / 32.0)
    freq_l = 10000.0 ** (-np.arange(16) / 16.0)
    freq = np.concatenate([freq_w, freq_w, freq_l, freq_l, np.zeros(32)])
    is_sin = np.concatenate(
        [np.zeros(32), np.ones(32), np.zeros(16), np.ones(16), np.zeros(32)]) > 0
    inner = np.arange(rows)[:, None] * freq[None]
    c, s = np.cos(inner), np.sin(inner)
    first = np.where(is_sin, s, c).astype(np.float32)
    second = np.where(is_sin, c, -s).astype(np.float32)
    outer = (np.arange(n_sp) * rows)[:, None] * freq[None]
    offs = np.stack([np.cos(outer), np.sin(outer)], axis=1).astype(np.float32)
    return first, second, offs


def shards(n_sp, n_tp, x, gain, lq, ld, rd, lgain, lu, wq, wk, wv, sink, ol, ow):
    rows, feat = x.shape
    nr = rows // CH
    nx = n_tp // 2
    heads = lu.shape[1] // (NOPE + HEAD)
    wheads = wq.shape[1] // HEAD
    kheads = wk.shape[1] // HEAD
    latent = ld.shape[1]
    dims = (n_sp, n_tp, rows, feat, heads, wheads, kheads)
    first, second, offs = tables(rows, n_sp)
    vm = pl.BlockSpec(memory_space=pltpu.VMEM)
    hb = pl.BlockSpec(memory_space=pl.ANY)
    big = [lq, ld, rd, lu, wq, wk, wv, ol, ow]
    dma = pltpu.SemaphoreType.DMA
    scratch = [pltpu.VMEM(a.shape, a.dtype) for a in big] + [
        pltpu.VMEM((n_tp, nr, CH, feat), BF16),
        pltpu.VMEM((CH, n_tp * feat), BF16),
        pltpu.VMEM((n_sp, nr, CH, latent), BF16),
        pltpu.VMEM((n_sp, nr, ROPE, CH), BF16),
        pltpu.VMEM((heads, rows, 128), BF16),
        pltpu.VMEM((wheads, rows, kheads * HEAD), BF16),
        pltpu.VMEM((nr + 2, CH, kheads * HEAD), BF16),
        pltpu.VMEM((nr + 2, CH, kheads * HEAD), BF16),
        pltpu.VMEM((heads, rows, 128), BF16),
        pltpu.VMEM((heads, rows, 128), BF16),
        pltpu.VMEM((heads, rows, 128), F32),
        pltpu.VMEM((heads, rows, 128), F32),
        pltpu.VMEM((rows, heads * HEAD), BF16),
        pltpu.VMEM((rows, wheads * HEAD), BF16),
        pltpu.VMEM((nx, nr, CH, feat), BF16),
        pltpu.VMEM((nx, nr, CH, feat), F32),
        pltpu.VMEM((nx, nr, CH, feat), BF16),
        pltpu.VMEM((nx, nr, CH, feat), BF16),
        pltpu.VMEM((nx, nr, CH, feat), BF16),
        dma((9,)),
        dma((nx, nr)), dma((n_tp, nr)), dma((nx, nr)),
        dma((2, n_sp, 2)), dma((n_sp, nr)), dma((n_sp, 2)),
        dma((2, n_sp, 2)), dma((n_sp, nr)), dma((n_sp, 2)),
        dma((2, 2)), dma((2, 2)),
        dma((nx, nr)), dma((nx, nr)), dma((nx, nr)), dma((nx, nr)),
    ]
    return pl.pallas_call(
        functools.partial(body, dims),
        out_shape=jax.ShapeDtypeStruct((rows, feat), BF16),
        in_specs=[vm, vm, hb, hb, hb, vm, hb, hb, hb, hb, vm, hb, hb, vm, vm, vm],
        out_specs=vm,
        scratch_shapes=scratch,
        compiler_params=pltpu.CompilerParams(
            collective_id=0, has_side_effects=True, vmem_limit_bytes=60 * 1024 * 1024),
    )(x, gain[None], lq, ld, rd, lgain[None], lu, wq, wk, wv, sink[None], ol, ow,
      jnp.asarray(first), jnp.asarray(second), jnp.asarray(offs))


def solution(mesh):
    in_specs = (
        P("sp", "tp"),
        P(),
        P(None, "tp"),
        P(),
        P(),
        P(),
        P(None, "tp"),
        P(None, "tp"),
        P(None, "tp"),
        P(None, "tp"),
        P("tp"),
        P("tp", None),
        P("tp", None),
    )
    step = functools.partial(shards, mesh.shape["sp"], mesh.shape["tp"])
    return jax.shard_map(
        step, mesh=mesh, in_specs=in_specs, out_specs=P("sp", "tp"), check_vma=False)
```

time: 244 us -> 99 us (0.41)
  Pallas kernels: 0 us -> 95.1 us
  matrix products: 76.4 us -> 0 us
  waiting for transfers between devices: 75.4 us -> 0 us
  blocking collectives: 33.9 us -> 0 us
  local copies, waits for them, and re-layouts: 23 us -> 3.78 us
  other arithmetic: 14.5 us -> 0 us
  between operations: 13.6 us -> 0.01 us
  starting transfers between devices: 5.35 us -> 0 us
    pallas_call x0 -> x1, Pallas kernels: none -> 95.1 us  [shards(): pl.pallas_call(functools.partial(body, dims), out_shape=jax.ShapeDtypeStr...]
    dot_general x35 -> x0, matrix products: 76.4 us -> none  [the longest x8 28.6 us: attend(): jnp.einsum('qhr,kr->hqk', queries[..., NOPE:], rope_keys, preferred_eleme...]
    all_gather x2 -> x0, waiting for transfers between devices: 44.6 us -> none  [the longest x1 26.9 us: shards(): gathered = lax.all_gather(inputs, 'tp', axis=1, tiled=True)]
    all_gather x1 -> x0, blocking collectives: 33.9 us -> none  [shards(): lax.all_gather(shared, 'sp', axis=0, tiled=True)]
    reduce_scatter x1 -> x0, waiting for transfers between devices: 30 us -> none  [shards(): lax.psum_scatter((lax.dot_general(out_latent, latent_out, contract_dims,...]
    dynamic_slice x16 -> x0, local copies, waits for them, and re-layouts: 10.3 us -> none  [attend_rows(): running, unused = lax.scan(advance, running, sliced)]
    reduce_sum x10 -> x0, other arithmetic: 7.53 us -> none  [the longest x8 4.61 us: attend(): denoms = denoms * shrink + jnp.sum(weights, axis=-1)]
    while x88 -> x0, local copies, waits for them, and re-layouts: 7.46 us -> none
  transfers between devices with their start and end apart: 5 -> 0, of which waited for: 3 -> 0; matrix products, arithmetic and copies ran while one was open for 8% -> 0% of each run, Pallas kernels for 0% -> 0%
where the time goes in v1:
time: 99 us; the launch traced here: 98.8 us
  Pallas kernels  95.1 us (96%)
  local copies, waits for them, and re-layouts  3.78 us (4%)
    pallas_call x1, Pallas kernels, shards(): pl.pallas_call(functools.partial(body, dims), out_shape=jax.ShapeDtypeStr...  95.1 us
    unnamed x2, local copies, waits for them, and re-layouts  3.78 us

profile of v1, /device:TPU:0, one launch (start us, length us, event | category | flops | bytes accessed | tf_op | source)
XLA Modules:
  0.0 98.8 jit_solution(14954337668249799066)
XLA Ops:
  0.0 1.9 %copy.17.refs_4_ = bf16[2048,32]{1,0:T(8,128)(2,1)} copy(bf16[2048,32]{0,1:T(8,128)(2,1)} %param.20) | data formatting | bytes 262144 | tf_op args[4]
  1.9 95.1 %shard_map.154 = bf16[512,512]{1,0:T(8,128)(2,1)} custom-call(bf16[512,512]{1,0:T(8,128)(2,1)} %refs_0_.1, f32[1,2048]{1,0:T(1,128)} %bitcast.3, bf16[2048,384]{1,0:T(8,128)(2,1)} %refs_2_.1, bf16[2048,512]{1,0:T(8,128)(2,1)} %refs_3_.1, bf16[2048,32]{1,0:T(8,128)(2,1)} %copy.17.refs_4_, f32[1,512]{1,0:T(1,128)} %bitcast.4, bf16[512,512]{1,0:T(8,128)(2,1)} %refs_6_.1, ...), custom_call_target="tpu_custom_call" | custom-call | tf_op jit(solution)/shard_map/pallas_call | solution.py:491
  97.0 1.9 %copy.19 = bf16[512,512]{1,0:T(8,128)(2,1)} copy(bf16[512,512]{1,0:T(8,128)(2,1)} %shard_map.154) | data formatting | bytes 1048576

commit v2 on v1

--- a/solution.py
+++ b/solution.py
@@ -58,7 +58,7 @@
     (x_ref, gain_ref, lq_h, ld_h, rd_h, lgain_ref, lu_h, wq_h, wk_h, wv_h, sink_ref,
      ol_h, ow_h, cp_ref, cq_ref, off_ref, out_ref,
      lq, ld, rd, lu, wq, wk, wv, ol, ow, xg, hid, lat, krt, qs, qw, wkb, wvb,
-     kop, vop, acc, mx, oml, omw, part_p, part_m, prec, xs, xr,
+     luk, kop, vop, acc, mx, oml, omw, part_p, part_m, prec, xs, xr,
      wsem, xsend, xrecv, xfsend, lsend, lrecv, lfsend, ksend, krecv, kfsend,
      hsend, hrecv, psend, precv, ssend, srecv) = refs
     nr = rows // CH
@@ -126,8 +126,14 @@
         return 0
 
     lax.fori_loop(0, nr, start_x, 0)
-    for w in weights[:6]:
+    acc[...] = jnp.zeros_like(acc)
+    mx[...] = jnp.full_like(mx, -1e30)
+    kop[...] = jnp.zeros_like(kop)
+    for w in weights[:7]:
         w.wait()
+    for h in range(heads):
+        luk[h * NOPE:(h + 1) * NOPE, :] = (
+            lu[:, h * 128:(h + 1) * 128].astype(F32).T[:NOPE].astype(BF16))
 
     def uslot(b, r):
         return lat.at[b, r], krt.at[b, r]
@@ -166,7 +172,8 @@
         low = jnp.dot(hid[...], ld[...], preferred_element_type=F32) * scale
         low = low * lax.rsqrt(jnp.mean(low * low, axis=-1, keepdims=True) + EPS) * lgain_ref[...]
         lat[sp, r] = low.astype(BF16)
-        shared = jnp.dot(hid[...], rd[...], preferred_element_type=F32) * scale
+        shared = lax.dot_general(hid[...], rd[...], (((1,), (1,)), ((), ())),
+                                 preferred_element_type=F32) * scale
         shared = rotate(shared, cos_l, sin_l)
         wide = jnp.concatenate([shared, jnp.zeros((CH, CH - ROPE), F32)], axis=-1)
         krt[sp, r] = wide.T[:ROPE].astype(BF16)
@@ -226,43 +233,40 @@
         return 0
 
     lax.fori_loop(0, nr + 1, gather_step, 0)
-    weights[6].wait()
-
-    acc[...] = jnp.zeros_like(acc)
-    mx[...] = jnp.full_like(mx, -1e30)
-    lane = lax.broadcasted_iota(jnp.int32, (CH, CH), 1)
+    lane = lax.broadcasted_iota(jnp.int32, (rows, 128), 1)
 
     def block(b):
-        def expand(r, _):
-            e = jnp.dot(lat[b, r], lu[...], preferred_element_type=F32)
-            kt = jnp.concatenate(
-                [jnp.zeros((NOPE, CH), F32), krt[b, r].astype(F32),
-                 jnp.zeros((128 - NOPE - ROPE, CH), F32)], axis=0).T
-            span = pl.ds(pl.multiple_of(r * CH, CH), CH)
-            for h in range(heads):
-                eh = e[:, h * 128:(h + 1) * 128]
-                kop[h, span, :] = jnp.where(lane < NOPE, eh, kt).astype(BF16)
-                vop[h, span, :] = jnp.where(lane < NOPE, 1.0, eh).astype(BF16)
-            return 0
-
-        lax.fori_loop(0, nr, expand, 0)
+        keys = lat[b].reshape(rows, lat.shape[-1])
+        et = lax.dot_general(luk[...], keys, (((1,), (1,)), ((), ())),
+                             preferred_element_type=F32).astype(BF16)
+        ev = jnp.dot(keys, lu[...], preferred_element_type=F32)
+        for h in range(heads):
+            kop[h, 0:NOPE, :] = et[h * NOPE:(h + 1) * NOPE]
+            for r in range(nr):
+                kop[h, NOPE:NOPE + ROPE, r * CH:(r + 1) * CH] = krt[b, r]
+            vop[h] = jnp.where(lane < NOPE, 1.0, ev[:, h * 128:(h + 1) * 128]).astype(BF16)
         qt = 256
         tiles = rows // qt
 
-        def tile(i, _):
-            h, t = i // tiles, i % tiles
+        def tile(t, _):
             span = pl.ds(pl.multiple_of(t * qt, qt), qt)
-            s = lax.dot_general(qs[h, span, :], kop[h], (((1,), (1,)), ((), ())),
-                                preferred_element_type=F32)
-            old = mx[h, span, :]
-            new = jnp.maximum(old, jnp.max(s, axis=-1, keepdims=True))
-            p = jnp.exp2(s - new[:, 0:1]).astype(BF16)
-            acc[h, span, :] = acc[h, span, :] * jnp.exp2(old - new) + jnp.dot(
-                p, vop[h], preferred_element_type=F32)
-            mx[h, span, :] = new
+
+            def score(h):
+                return jnp.dot(qs[h, span, :], kop[h], preferred_element_type=F32)
+
+            s = score(0)
+            for h in range(heads):
+                ahead = score(h + 1) if h + 1 < heads else None
+                old = mx[h, span, :]
+                new = jnp.maximum(old, jnp.max(s, axis=-1, keepdims=True))
+                p = jnp.exp2(s - jnp.concatenate([new] * (rows // 128), axis=-1)).astype(BF16)
+                acc[h, span, :] = acc[h, span, :] * jnp.exp2(old - new) + jnp.dot(
+                    p, vop[h], preferred_element_type=F32)
+                mx[h, span, :] = new
+                s = ahead
             return 0
 
-        lax.fori_loop(0, heads * tiles, tile, 0)
+        lax.fori_loop(0, tiles, tile, 0)
 
     def window():
         for i in range(2):
@@ -459,6 +463,7 @@
     first, second, offs = tables(rows, n_sp)
     vm = pl.BlockSpec(memory_space=pltpu.VMEM)
     hb = pl.BlockSpec(memory_space=pl.ANY)
+    rd = rd.T
     big = [lq, ld, rd, lu, wq, wk, wv, ol, ow]
     dma = pltpu.SemaphoreType.DMA
     scratch = [pltpu.VMEM(a.shape, a.dtype) for a in big] + [
@@ -470,7 +475,8 @@
         pltpu.VMEM((wheads, rows, kheads * HEAD), BF16),
         pltpu.VMEM((nr + 2, CH, kheads * HEAD), BF16),
         pltpu.VMEM((nr + 2, CH, kheads * HEAD), BF16),
-        pltpu.VMEM((heads, rows, 128), BF16),
+        pltpu.VMEM((heads * NOPE, latent), BF16),
+        pltpu.VMEM((heads, 128, rows), BF16),
         pltpu.VMEM((heads, rows, 128), BF16),
         pltpu.VMEM((heads, rows, 128), F32),
         pltpu.VMEM((heads, rows, 128), F32),

time: 99 us -> 74.6 us (0.75)
  Pallas kernels: 95.1 us -> 72.5 us
  local copies, waits for them, and re-layouts: 3.78 us -> 1.87 us
    pallas_call x1, Pallas kernels: 95.1 us -> 72.5 us  [shards(): pl.pallas_call(functools.partial(body, dims), out_shape=jax.ShapeDtypeStr...]
    unnamed x2 -> x1, local copies, waits for them, and re-layouts: 3.78 us -> 1.87 us
where the time goes in v2:
time: 74.6 us; the launch traced here: 74.4 us
  Pallas kernels  72.5 us (97%)
  local copies, waits for them, and re-layouts  1.87 us (3%)
    pallas_call x1, Pallas kernels, shards(): pl.pallas_call(functools.partial(body, dims), out_shape=jax.ShapeDtypeStr...  72.5 us
    unnamed x1, local copies, waits for them, and re-layouts  1.87 us

profile of v2, /device:TPU:0, one launch (start us, length us, event | category | flops | bytes accessed | tf_op | source)
XLA Modules:
  0.0 74.4 jit_solution(16894668582013628426)
XLA Ops:
  0.0 72.5 %shard_map.154 = bf16[512,512]{1,0:T(8,128)(2,1)} custom-call(bf16[512,512]{1,0:T(8,128)(2,1)} %refs_0_.1, f32[1,2048]{1,0:T(1,128)} %bitcast.5, bf16[2048,384]{1,0:T(8,128)(2,1)} %refs_2_.1, bf16[2048,512]{1,0:T(8,128)(2,1)} %refs_3_.1, bf16[32,2048]{1,0:T(8,128)(2,1)} %bitcast.4, f32[1,512]{1,0:T(1,128)} %bitcast.6, bf16[512,512]{1,0:T(8,128)(2,1)} %refs_6_.1, ...), custom_call_target="tpu_custom_call" | custom-call | tf_op jit(solution)/shard_map/pallas_call | solution.py:497
  72.5 1.9 %copy.18 = bf16[512,512]{1,0:T(8,128)(2,1)} copy(bf16[512,512]{1,0:T(8,128)(2,1)} %shard_map.154) | data formatting | bytes 1048576
